TPU v7x, 32 devices: a whole 2x2x4 slice. The times are simulated.
32 devices in a mesh: kv: 8 (over z, y), tp: 4 (over x, core).
Axes of the slice: x: 2, y: 2, z: 4, core: 2. Of those that a mesh axis runs over, the one named last changes fastest.
Arguments:
- tokens: bfloat16 [4096, 2048], P('kv'), may hold values from -18 to 18
- w_query: bfloat16 [2048, 1024], P(None, 'tp'), may hold values from -0.125 to 0.125
- w_key: bfloat16 [2048, 256], P(None, 'tp'), may hold values from -0.125 to 0.125
- w_value: bfloat16 [2048, 256], P(None, 'tp'), may hold values from -18 to 18
- w_out: bfloat16 [1024, 2048], P(None, 'tp'), may hold values from -0.1875 to 0.1875
- out_gain: float32 [1024], replicated, may hold values from 0.1 to 1.9
- chosen: int32 [4, 64, 8], P('tp', 'kv'), may hold values from -1 to 63, as said below
Outputs:
- mixed_out: bfloat16 [4096, 2048], P('kv', 'tp')
Inputs may be any that keep to these rules, and one draw needn't show every extreme that they name: chosen[h, b, 0] is b itself; the other entries of a row are distinct key blocks lying wholly before block b, or -1, placed after all named blocks; for each key head h, the query blocks on one index of kv (its 512 positions) name, together, at most one key block of head h held by any other index of kv.
All inputs are finite; a program needn't handle non-finite values.
Results may differ from a plain program's by a relative error of at most 0.024.
Values may be sent and summed in bfloat16 or wider, within the bound.
No kernel may reach another device: no remote copies, remote signals or barrier semaphores. Data moves between devices by JAX's collectives and lax.ppermute only.
A program may use at most 64 MiB of HBM per device.

v0:
```python
import jax
import jax.numpy as jnp
from jax import lax
from jax.sharding import PartitionSpec as P

HQ = 16
HD = 64
BLK = 64
SEL = 8
rope_base = 500000.0
norm_eps = 1e-06


def rotate(vectors, positions):
    half_size = vectors.shape[-1] // 2
    frequency = rope_base ** (-jnp.arange(half_size, dtype=jnp.float32) / half_size)
    angles = positions.astype(jnp.float32)[:, None] * frequency[None, :]
    cosine = jnp.cos(angles)[:, None, :]
    sine_wave = jnp.sin(angles)[:, None, :]
    lower_half = vectors[..., :half_size]
    upper_half = vectors[..., half_size:]
    return jnp.concatenate(
        [
            lower_half * cosine - upper_half * sine_wave,
            upper_half * cosine + lower_half * sine_wave,
        ],
        axis=-1,
    )


def per_device(tokens, w_query, w_key, w_value, w_out, out_gain, chosen):
    count_kv = lax.axis_size("kv")
    kv_place = lax.axis_index("kv")
    row_count = tokens.shape[0]
    block_count = row_count // BLK
    feat_width = w_query.shape[1]
    head_count = feat_width // HD
    positions = kv_place * row_count + jnp.arange(row_count, dtype=jnp.int32)
    queries = rotate(
        jnp.dot(tokens, w_query, preferred_element_type=jnp.float32).reshape(
            row_count, head_count, HD
        ),
        positions,
    ).astype(jnp.bfloat16)
    key_rows = (
        rotate(
            jnp.dot(tokens, w_key, preferred_element_type=jnp.float32).reshape(row_count, 1, HD),
            positions,
        )
        .astype(jnp.bfloat16)
        .reshape(row_count, HD)
    )
    value_rows = jnp.dot(tokens, w_value, preferred_element_type=jnp.float32).astype(jnp.bfloat16)
    local_pairs = jnp.concatenate([key_rows, value_rows], axis=1).reshape(block_count, BLK, 2 * HD)
    chosen_ids = chosen[0]
    usable = chosen_ids >= 0
    owners = jnp.where(usable, chosen_ids // block_count, kv_place)
    local_index = jnp.where(usable, chosen_ids % block_count, 0)
    remote = usable & (owners != kv_place)
    peer_ids = jnp.arange(count_kv, dtype=jnp.int32)
    matches = remote[:, :, None] & (owners[:, :, None] == peer_ids[None, None, :])
    wanted = jnp.max(jnp.where(matches, local_index[:, :, None], -1), axis=(0, 1))
    asked_for = lax.all_to_all(
        wanted.reshape(count_kv, 1), "kv", split_axis=0, concat_axis=0, tiled=True
    )[:, 0]
    outgoing = jnp.where(
        (asked_for >= 0)[:, None, None],
        local_pairs[jnp.maximum(asked_for, 0)],
        jnp.zeros((), jnp.bfloat16),
    )
    arrived = lax.all_to_all(outgoing, "kv", split_axis=0, concat_axis=0, tiled=True)
    pool_pairs = jnp.concatenate([arrived, local_pairs], axis=0)
    slot_index = jnp.where(owners == kv_place, count_kv + local_index, owners)
    selected = pool_pairs[slot_index]
    pair_count = block_count // 2
    offsets = jnp.arange(BLK, dtype=jnp.int32)
    score_scale = HD ** (-0.5)

    def attend(bundle):
        query_part, stacked, pair_ids, pair_usable, query_pos = bundle
        key_part = stacked[..., :HD]
        value_part = stacked[..., HD:]
        scores = (
            jnp.einsum("pqhd,pskd->phqsk", query_part, key_part, preferred_element_type=jnp.float32)
            * score_scale
        )
        key_pos = pair_ids[:, :, None] * BLK + offsets
        allowed = pair_usable[:, None, :, None] & (
            key_pos[:, None, :, :] <= query_pos[:, :, None, None]
        )
        scores = jnp.where(allowed[:, None], scores, -jnp.inf)
        peak_score = jnp.max(scores, axis=(3, 4), keepdims=True)
        weights = jnp.exp(scores - peak_score)
        softmax_w = (weights / jnp.sum(weights, axis=(3, 4), keepdims=True)).astype(jnp.bfloat16)
        mixed_out = jnp.einsum(
            "phqsk,pskd->pqhd", softmax_w, value_part, preferred_element_type=jnp.float32
        )
        return mixed_out.astype(jnp.bfloat16)

    attended = lax.map(
        attend,
        (
            queries.reshape(pair_count, 2, BLK, head_count, HD),
            selected.reshape(pair_count, 2, SEL, BLK, 2 * HD),
            chosen_ids.reshape(pair_count, 2, SEL),
            usable.reshape(pair_count, 2, SEL),
            positions.reshape(pair_count, 2, BLK),
        ),
    ).reshape(row_count, feat_width)
    attn_f32 = attended.astype(jnp.float32)
    squares = lax.psum(jnp.sum(attn_f32 * attn_f32, axis=1), "tp")
    gain_part = lax.dynamic_slice_in_dim(out_gain, lax.axis_index("tp") * feat_width, feat_width)
    scaled = (attn_f32 * gain_part[None, :]).astype(jnp.bfloat16)
    product = jnp.dot(
        lax.all_gather(scaled, "tp", axis=1, tiled=True), w_out, preferred_element_type=jnp.float32
    )
    inverse = lax.rsqrt(squares / (HQ * HD) + norm_eps)
    return (inverse[:, None] * product).astype(jnp.bfloat16)


def solution(mesh):
    return jax.shard_map(
        per_device,
        mesh=mesh,
        in_specs=(
            P("kv", None),
            P(None, "tp"),
            P(None, "tp"),
            P(None, "tp"),
            P(None, "tp"),
            P(),
            P("tp", "kv", None),
        ),
        out_specs=P("kv", "tp"),
        check_vma=False,
    )
```

profile of v0, /device:TPU:0, one launch (start us, length us, event | category | flops | bytes accessed | tf_op | source)
XLA Modules:
  0.0 87.1 jit_solution(12271367534152278380)
XLA Ops:
  6.5 0.8 fusion.20
  8.9 7.3 %all-to-all-start = ((s32[8,1,1]{2,1,0:T(1,128)}), s32[8,1,1]{2,1,0:T(1,128)S(1)}, u32[]{:S(2)}, u32[]{:S(2)}) async-start(s32[8,1,1]{2,1,0:T(1,128)} %copy.36), calls=%async_computation | async-start | bytes 8192 | tf_op jit(solution)/shard_map/all_to_all | solution.py:63
  16.9 1.7 %convolution_bitcast_fusion.1 = f32[512,1,64]{0,2,1:T(8,128)S(1)} fusion(bf16[512,2048]{1,0:T(8,128)(2,1)S(1)} %copy-done, bf16[2048,64]{0,1:T(8,128)(2,1)} %param.11), kind=kOutput, calls=%fused_computation.26 | convolution fusion | flops 134217728 | bytes 2490368 | tf_op jit(solution)/shard_map/dot_general | solution.py:47
  20.4 2.0 %fusion.34 = f32[512,256]{0,1:T(8,128)S(1)} fusion(bf16[512,2048]{1,0:T(8,128)(2,1)S(1)} %copy-done, bf16[2048,256]{1,0:T(8,128)(2,1)} %param.10), kind=kOutput, calls=%fused_computation.93 | convolution fusion | flops 536870912 | bytes 3670016 | tf_op jit(solution)/shard_map/dot_general | solution.py:40
  22.9 1.6 %pad_maximum_fusion = bf16[4,2,64,4,64]{2,1,0,4,3:T(2,128)(2,1)} fusion(bf16[4,2,64,4,32]{2,1,0,4,3:T(2,128)(2,1)S(1)} %concatenate.35, bf16[4,2,64,4,32]{2,1,0,4,3:T(2,128)(2,1)S(1)} %concatenate.34), kind=kLoop, calls=%fused_computation.29 | loop fusion | flops 131072 | bytes 524288 | tf_op jit(solution)/shard_map/concatenate | solution.py:22
  26.6 6.0 %all-to-all-start.1 = ((bf16[8,64,128]{2,1,0:T(8,128)(2,1)}), bf16[8,64,128]{2,1,0:T(8,128)(2,1)S(1)}, u32[]{:S(2)}, u32[]{:S(2)}) async-start(bf16[8,64,128]{2,1,0:T(8,128)(2,1)} %broadcast_select_fusion), calls=%async_computation.1 | async-start | bytes 262144 | tf_op jit(solution)/shard_map/all_to_all | solution.py:71
  32.7 0.8 dynamic_slice.23
  33.4 6.5 %all-to-all-done.1 = bf16[8,64,128]{2,1,0:T(8,128)(2,1)S(1)} async-done(((bf16[8,64,128]{2,1,0:T(8,128)(2,1)}), bf16[8,64,128]{2,1,0:T(8,128)(2,1)S(1)}, u32[]{:S(2)}, u32[]{:S(2)}) %all-to-all-start.1) | async-done | bytes 131104 | tf_op jit(solution)/shard_map/all_to_all | solution.py:71
  40.8 17.1 %while.11 = (s32[]{:T(128)}, bf16[4,2,64,4,64]{2,4,3,1,0:T(8,128)(2,1)}, bf16[4,2,8,64,128]{4,3,2,1,0:T(8,128)(2,1)S(1)}, pred[4,2,8]{2,1,0:T(4,128)(4,1)S(1)}, ...) while((s32[]{:T(128)}, ...), condition=%wide.region_4.5_spmd.clone, body=%wide.region_1.4_spmd.clone.sunk | while | flops 69369872 | bytes 13193617 | solution.py:100
  41.8 1.0 %constant_dynamic-slice_fusion.4 = bf16[1,2,64,4,64]{2,1,0,4,3:T(2,128)(2,1)S(1)} fusion(bf16[4,2,64,4,64]{2,1,0,4,3:T(2,128)(2,1)} %get-tuple-element.185, s32[]{:T(128)} %get-tuple-element.171), kind=kLoop, calls=%fused_computation.18.clone.1 | loop fusion | bytes 131076 | tf_op jit(solution)/shard_map/while/body/jit(dynamic_index_in_dim)/dynamic_slice | solution.py:100
  43.9 1.2 %fusion.52 = bf16[4,2,64,4,64]{2,4,3,1,0:T(8,128)(2,1)} fusion(bf16[4,2,64,4,64]{2,4,3,1,0:T(8,128)(2,1)} %get-tuple-element.172, s32[]{:T(128)} %get-tuple-element.171, f32[2,4,64,8,64]{2,4,1,3,0:T(8,128)S(1)} %get-tuple-element.161, f32[2,4,64]{2,1,0:T(4,128)S(1)} %fusion.51, f32[2,4,64]{2,1,0:T(4,128)S(1)} %get-tuple-element.162, ...), kind=kOutput, calls=%fused_computation.10.clone.1 | convolution fusion | flops 34373632 | bytes 1446400 | tf_op jit(solution)/shard_map/while/body/eval_jaxpr/phqsk,pskd->pqhd/dot_general | solution.py:95
  46.1 1.0 %constant_dynamic-slice_fusion.4 = bf16[1,2,64,4,64]{2,1,0,4,3:T(2,128)(2,1)S(1)} fusion(bf16[4,2,64,4,64]{2,1,0,4,3:T(2,128)(2,1)} %get-tuple-element.185, s32[]{:T(128)} %get-tuple-element.171), kind=kLoop, calls=%fused_computation.18.clone.1 | loop fusion | bytes 131076 | tf_op jit(solution)/shard_map/while/body/jit(dynamic_index_in_dim)/dynamic_slice | solution.py:100
  48.1 1.2 %fusion.52 = bf16[4,2,64,4,64]{2,4,3,1,0:T(8,128)(2,1)} fusion(bf16[4,2,64,4,64]{2,4,3,1,0:T(8,128)(2,1)} %get-tuple-element.172, s32[]{:T(128)} %get-tuple-element.171, f32[2,4,64,8,64]{2,4,1,3,0:T(8,128)S(1)} %get-tuple-element.161, f32[2,4,64]{2,1,0:T(4,128)S(1)} %fusion.51, f32[2,4,64]{2,1,0:T(4,128)S(1)} %get-tuple-element.162, ...), kind=kOutput, calls=%fused_computation.10.clone.1 | convolution fusion | flops 34373632 | bytes 1446400 | tf_op jit(solution)/shard_map/while/body/eval_jaxpr/phqsk,pskd->pqhd/dot_general | solution.py:95
  50.4 1.0 %constant_dynamic-slice_fusion.4 = bf16[1,2,64,4,64]{2,1,0,4,3:T(2,128)(2,1)S(1)} fusion(bf16[4,2,64,4,64]{2,1,0,4,3:T(2,128)(2,1)} %get-tuple-element.185, s32[]{:T(128)} %get-tuple-element.171), kind=kLoop, calls=%fused_computation.18.clone.1 | loop fusion | bytes 131076 | tf_op jit(solution)/shard_map/while/body/jit(dynamic_index_in_dim)/dynamic_slice | solution.py:100
  52.4 1.2 %fusion.52 = bf16[4,2,64,4,64]{2,4,3,1,0:T(8,128)(2,1)} fusion(bf16[4,2,64,4,64]{2,4,3,1,0:T(8,128)(2,1)} %get-tuple-element.172, s32[]{:T(128)} %get-tuple-element.171, f32[2,4,64,8,64]{2,4,1,3,0:T(8,128)S(1)} %get-tuple-element.161, f32[2,4,64]{2,1,0:T(4,128)S(1)} %fusion.51, f32[2,4,64]{2,1,0:T(4,128)S(1)} %get-tuple-element.162, ...), kind=kOutput, calls=%fused_computation.10.clone.1 | convolution fusion | flops 34373632 | bytes 1446400 | tf_op jit(solution)/shard_map/while/body/eval_jaxpr/phqsk,pskd->pqhd/dot_general | solution.py:95
  54.7 1.0 %constant_dynamic-slice_fusion.4 = bf16[1,2,64,4,64]{2,1,0,4,3:T(2,128)(2,1)S(1)} fusion(bf16[4,2,64,4,64]{2,1,0,4,3:T(2,128)(2,1)} %get-tuple-element.185, s32[]{:T(128)} %get-tuple-element.171), kind=kLoop, calls=%fused_computation.18.clone.1 | loop fusion | bytes 131076 | tf_op jit(solution)/shard_map/while/body/jit(dynamic_index_in_dim)/dynamic_slice | solution.py:100
  56.7 1.2 %fusion.52 = bf16[4,2,64,4,64]{2,4,3,1,0:T(8,128)(2,1)} fusion(bf16[4,2,64,4,64]{2,4,3,1,0:T(8,128)(2,1)} %get-tuple-element.172, s32[]{:T(128)} %get-tuple-element.171, f32[2,4,64,8,64]{2,4,1,3,0:T(8,128)S(1)} %get-tuple-element.161, f32[2,4,64]{2,1,0:T(4,128)S(1)} %fusion.51, f32[2,4,64]{2,1,0:T(4,128)S(1)} %get-tuple-element.162, ...), kind=kOutput, calls=%fused_computation.10.clone.1 | convolution fusion | flops 34373632 | bytes 1446400 | tf_op jit(solution)/shard_map/while/body/eval_jaxpr/phqsk,pskd->pqhd/dot_general | solution.py:95
  57.9 1.3 %copy.41 = f32[4,2,64,4,64]{4,3,2,1,0:T(4,128)S(1)} copy(bf16[4,2,64,4,64]{2,4,3,1,0:T(8,128)(2,1)} %get-tuple-element.47) | data formatting | bytes 786432 | tf_op jit(solution)/shard_map/convert_element_type | solution.py:110
  59.3 1.4 %reshape.350 = f32[512,256]{1,0:T(8,128)} reshape(f32[4,2,64,4,64]{4,3,2,1,0:T(4,128)S(1)} %copy.41) | data formatting | bytes 1048576 | tf_op jit(solution)/shard_map/convert_element_type | solution.py:110
  60.7 1.8 %multiply_convert_fusion = bf16[512,256]{1,0:T(8,128)(2,1)} fusion(f32[512,256]{1,0:T(8,128)} %reshape.350, f32[256]{0:T(256)S(1)} %dynamic_slice.23), kind=kLoop, calls=%fused_computation.30 | loop fusion | flops 262144 | bytes 787456 | tf_op jit(solution)/shard_map/convert_element_type | solution.py:113
  62.5 1.2 %multiply_reduce_fusion = f32[4,2,64]{2,1,0:T(2,128)S(1)} fusion(bf16[4,2,64,4,64]{2,4,3,1,0:T(8,128)(2,1)} %get-tuple-element.47), kind=kLoop, calls=%fused_computation.28 | loop fusion | flops 392704 | bytes 264192 | tf_op jit(solution)/shard_map/reduce_sum | solution.py:111
  63.8 5.6 %psum.7 = f32[512]{0:T(512)S(1)} all-reduce(f32[512]{0:T(512)S(1)} %reduce_sum.21), channel_id=1, replica_groups=mesh['kv'=8,'tp'=4] {'tp'}, use_global_device_ids=true, to_apply=%region_6.7 | all-reduce | flops 512 | bytes 4096 | tf_op jit(solution)/shard_map/psum | solution.py:111
  69.4 7.8 %all-gather.2.cloned.1.call-done = bf16[512,1024]{1,0:T(8,128)(2,1)} async-done(((bf16[512,256]{1,0:T(8,128)(2,1)}), bf16[512,1024]{1,0:T(8,128)(2,1)}) %all-gather.2.cloned.1.call-update) | async-done | bytes 1048592 | tf_op jit(solution)/shard_map/all_gather | solution.py:115
  77.3 3.0 %fusion.10 = bf16[512,512]{1,0:T(8,128)(2,1)} fusion(bf16[512,1024]{1,0:T(8,128)(2,1)} %all-gather.2.cloned.1.call-done, bf16[1024,512]{1,0:T(8,128)(2,1)} %param.13, f32[512]{0:T(512)S(1)} %add_rsqrt_fusion), kind=kOutput, calls=%fused_computation.25 | convolution fusion | flops 537395200 | bytes 2623488 | tf_op jit(solution)/shard_map/dot_general | solution.py:114
  (91 shorter events, 15.5 us)
Async XLA Ops:
  6.5 10.4 %copy-start = (bf16[512,2048]{1,0:T(8,128)(2,1)S(1)}, bf16[512,2048]{1,0:T(8,128)(2,1)}, u32[]{:S(2)}) copy-start(bf16[512,2048]{1,0:T(8,128)(2,1)} %param.9) | copy-start | bytes 6291460
  6.5 13.0 %copy-start.3 = (bf16[2048,64]{0,1:T(8,128)(2,1)S(1)}, bf16[2048,64]{0,1:T(8,128)(2,1)}, u32[]{:S(2)}) copy-start(bf16[2048,64]{0,1:T(8,128)(2,1)} %param.12) | copy-start | bytes 786436
  8.9 15.9 %all-to-all-start = ((s32[8,1,1]{2,1,0:T(1,128)}), s32[8,1,1]{2,1,0:T(1,128)S(1)}, u32[]{:S(2)}, u32[]{:S(2)}) async-start(s32[8,1,1]{2,1,0:T(1,128)} %copy.36), calls=%async_computation | async-start | bytes 8192 | tf_op jit(solution)/shard_map/all_to_all | solution.py:63
  22.4 11.0 %copy-start.4 = (s32[1,8,8]{2,1,0:T(8,128)S(1)}, s32[1,8,8]{2,1,0:T(8,128)}, u32[]{:S(2)}) copy-start(s32[1,8,8]{2,1,0:T(8,128)} %param.15) | copy-start | bytes 772
  26.6 13.3 %all-to-all-start.1 = ((bf16[8,64,128]{2,1,0:T(8,128)(2,1)}), bf16[8,64,128]{2,1,0:T(8,128)(2,1)S(1)}, u32[]{:S(2)}, u32[]{:S(2)}) async-start(bf16[8,64,128]{2,1,0:T(8,128)(2,1)} %broadcast_select_fusion), calls=%async_computation.1 | async-start | bytes 262144 | tf_op jit(solution)/shard_map/all_to_all | solution.py:71
  32.6 44.7 %all-gather.2.cloned.1.call-start = ((), (), s32[]{:S(2)}) async-start(), calls=%async_computation.2 | async-start | bytes 1310720 | tf_op jit(solution)/shard_map/all_gather | solution.py:115
  40.8 1.0 %copy-start.1 = (bf16[4,2,8,64,128]{4,3,2,1,0:T(8,128)(2,1)}, bf16[4,2,8,64,128]{4,3,2,1,0:T(8,128)(2,1)S(1)}, u32[]{:S(2)}) copy-start(bf16[4,2,8,64,128]{4,3,2,1,0:T(8,128)(2,1)S(1)} %get-tuple-element.181) | copy-start | bytes 3145732 | tf_op jit(solution)/shard_map/while
  43.9 1.2 %copy-start.2 = (bf16[4,2,8,64,128]{4,3,2,1,0:T(8,128)(2,1)S(1)}, bf16[4,2,8,64,128]{4,3,2,1,0:T(8,128)(2,1)}, u32[]{:S(2)}) copy-start(bf16[4,2,8,64,128]{4,3,2,1,0:T(8,128)(2,1)} %copy-done.1) | copy-start | bytes 3145732 | tf_op jit(solution)/shard_map/while
  45.1 1.0 %copy-start.1 = (bf16[4,2,8,64,128]{4,3,2,1,0:T(8,128)(2,1)}, bf16[4,2,8,64,128]{4,3,2,1,0:T(8,128)(2,1)S(1)}, u32[]{:S(2)}) copy-start(bf16[4,2,8,64,128]{4,3,2,1,0:T(8,128)(2,1)S(1)} %get-tuple-element.181) | copy-start | bytes 3145732 | tf_op jit(solution)/shard_map/while
  48.1 1.2 %copy-start.2 = (bf16[4,2,8,64,128]{4,3,2,1,0:T(8,128)(2,1)S(1)}, bf16[4,2,8,64,128]{4,3,2,1,0:T(8,128)(2,1)}, u32[]{:S(2)}) copy-start(bf16[4,2,8,64,128]{4,3,2,1,0:T(8,128)(2,1)} %copy-done.1) | copy-start | bytes 3145732 | tf_op jit(solution)/shard_map/while
  49.4 1.0 %copy-start.1 = (bf16[4,2,8,64,128]{4,3,2,1,0:T(8,128)(2,1)}, bf16[4,2,8,64,128]{4,3,2,1,0:T(8,128)(2,1)S(1)}, u32[]{:S(2)}) copy-start(bf16[4,2,8,64,128]{4,3,2,1,0:T(8,128)(2,1)S(1)} %get-tuple-element.181) | copy-start | bytes 3145732 | tf_op jit(solution)/shard_map/while
  52.4 1.2 %copy-start.2 = (bf16[4,2,8,64,128]{4,3,2,1,0:T(8,128)(2,1)S(1)}, bf16[4,2,8,64,128]{4,3,2,1,0:T(8,128)(2,1)}, u32[]{:S(2)}) copy-start(bf16[4,2,8,64,128]{4,3,2,1,0:T(8,128)(2,1)} %copy-done.1) | copy-start | bytes 3145732 | tf_op jit(solution)/shard_map/while
  53.7 1.0 %copy-start.1 = (bf16[4,2,8,64,128]{4,3,2,1,0:T(8,128)(2,1)}, bf16[4,2,8,64,128]{4,3,2,1,0:T(8,128)(2,1)S(1)}, u32[]{:S(2)}) copy-start(bf16[4,2,8,64,128]{4,3,2,1,0:T(8,128)(2,1)S(1)} %get-tuple-element.181) | copy-start | bytes 3145732 | tf_op jit(solution)/shard_map/while
  56.7 1.2 %copy-start.2 = (bf16[4,2,8,64,128]{4,3,2,1,0:T(8,128)(2,1)S(1)}, bf16[4,2,8,64,128]{4,3,2,1,0:T(8,128)(2,1)}, u32[]{:S(2)}) copy-start(bf16[4,2,8,64,128]{4,3,2,1,0:T(8,128)(2,1)} %copy-done.1) | copy-start | bytes 3145732 | tf_op jit(solution)/shard_map/while
Sparse Core Ops, SparseCore 0:
  62.6 14.5 all-gather.1
where the time goes:
time: 87.9 us; the launch traced here: 87.1 us
  matrix products  14.5 us (16%)
  waiting for transfers between devices  14.3 us (16%)
  local copies, waits for them, and re-layouts  13.6 us (15%)
  between operations  13.6 us (15%)
  starting transfers between devices  13.3 us (15%)
  other arithmetic  11.9 us (14%)
  blocking collectives  5.63 us (6%)
    all_gather x1, waiting for transfers between devices, per_device(): lax.all_gather(scaled, 'tp', axis=1, tiled=True)  7.83 us
    all_to_all x1, starting transfers between devices, per_device(): lax.all_to_all(wanted.reshape(count_kv, 1), 'kv', split_axis=0, concat_ax...  7.31 us
    all_to_all x1, waiting for transfers between devices, per_device(): lax.all_to_all(outgoing, 'kv', split_axis=0, concat_axis=0, tiled=True)  6.5 us
    all_to_all x1, starting transfers between devices, per_device(): lax.all_to_all(outgoing, 'kv', split_axis=0, concat_axis=0, tiled=True)  6 us
    psum x1, blocking collectives, per_device(): squares = lax.psum(jnp.sum(attn_f32 * attn_f32, axis=1), 'tp')  5.63 us
    dot_general x4, matrix products, attend(): jnp.einsum('phqsk,pskd->pqhd', softmax_w, value_part, preferred_element_t...  4.94 us
    dynamic_slice x8, local copies, waits for them, and re-layouts, per_device(): lax.map(attend, (queries.reshape(pair_count, 2, BLK, head_count, HD), sel...  4.53 us
    dot_general x1, matrix products, per_device(): jnp.dot(lax.all_gather(scaled, 'tp', axis=1, tiled=True), w_out, preferre...  3.04 us
  transfers between devices with their start and end apart: 3, of which 2 were waited for; matrix products, arithmetic and copies ran while one was open for 12% of the time, Pallas kernels for 0%

commit v1 on v0

--- a/solution.py
+++ b/solution.py
@@ -112,7 +112,11 @@
     gain_part = lax.dynamic_slice_in_dim(out_gain, lax.axis_index("tp") * feat_width, feat_width)
     scaled = (attn_f32 * gain_part[None, :]).astype(jnp.bfloat16)
     product = jnp.dot(
-        lax.all_gather(scaled, "tp", axis=1, tiled=True), w_out, preferred_element_type=jnp.float32
+        jnp.concatenate(
+            lax.all_to_all(jnp.stack([scaled] * lax.axis_size("tp")), "tp", 0, 0), axis=1
+        ),
+        w_out,
+        preferred_element_type=jnp.float32,
     )
     inverse = lax.rsqrt(squares / (HQ * HD) + norm_eps)
     return (inverse[:, None] * product).astype(jnp.bfloat16)

time: 87.9 us -> 79.4 us (0.903)
  between operations: 13.6 us -> 0.18 us
  blocking collectives: 5.63 us -> 14.6 us
  waiting for transfers between devices: 14.3 us -> 6.55 us
  starting transfers between devices: 13.3 us -> 16.8 us
  local copies, waits for them, and re-layouts: 13.6 us -> 14.8 us
    psum x1, blocking collectives: 5.63 us -> 14.6 us  [per_device(): squares = lax.psum(jnp.sum(attn_f32 * attn_f32, axis=1), 'tp')]
    all_gather x1 -> x0, waiting for transfers between devices: 7.83 us -> none  [per_device(): lax.all_gather(scaled, 'tp', axis=1, tiled=True)]
    all_to_all x0 -> x1, starting transfers between devices: none -> 3.51 us  [per_device(): lax.all_to_all(jnp.stack([scaled] * lax.axis_size('tp')), 'tp', 0, 0)]
    another operation x0 -> x1, local copies, waits for them, and re-layouts: none -> 1.07 us  [per_device(): jnp.stack([scaled] * lax.axis_size('tp'))]
  transfers between devices with their start and end apart: 3 -> 3, of which waited for: 2 -> 1; matrix products, arithmetic and copies ran while one was open for 12% -> 13% of each run, Pallas kernels for 0% -> 0%
where the time goes in v1:
time: 79.4 us; the launch traced here: 78.6 us
  starting transfers between devices  16.8 us (21%)
  local copies, waits for them, and re-layouts  14.8 us (19%)
  blocking collectives  14.6 us (18%)
  matrix products  14.3 us (18%)
  other arithmetic  11.2 us (14%)
  waiting for transfers between devices  6.55 us (8%)
    psum x1, blocking collectives, per_device(): squares = lax.psum(jnp.sum(attn_f32 * attn_f32, axis=1), 'tp')  14.6 us
    all_to_all x1, starting transfers between devices, per_device(): lax.all_to_all(wanted.reshape(count_kv, 1), 'kv', split_axis=0, concat_ax...  7.31 us
    all_to_all x1, waiting for transfers between devices, per_device(): lax.all_to_all(outgoing, 'kv', split_axis=0, concat_axis=0, tiled=True)  6.55 us
    all_to_all x1, starting transfers between devices, per_device(): lax.all_to_all(outgoing, 'kv', split_axis=0, concat_axis=0, tiled=True)  6 us
    dot_general x4, matrix products, attend(): jnp.einsum('phqsk,pskd->pqhd', softmax_w, value_part, preferred_element_t...  4.94 us
    dynamic_slice x8, local copies, waits for them, and re-layouts, per_device(): lax.map(attend, (queries.reshape(pair_count, 2, BLK, head_count, HD), sel...  4.53 us
    all_to_all x1, starting transfers between devices, per_device(): lax.all_to_all(jnp.stack([scaled] * lax.axis_size('tp')), 'tp', 0, 0)  3.51 us
    dot_general x1, matrix products, per_device(): jnp.dot(jnp.concatenate(lax.all_to_all(jnp.stack([scaled] * lax.axis_size...  2.76 us
  transfers between devices with their start and end apart: 3, of which 1 were waited for; matrix products, arithmetic and copies ran while one was open for 13% of the time, Pallas kernels for 0%

profile of v1, /device:TPU:0, one launch (start us, length us, event | category | flops | bytes accessed | tf_op | source)
XLA Modules:
  0.0 78.6 jit_solution(3233516566520393415)
XLA Ops:
  0.0 0.8 %fusion.20 = (s32[8,8]{1,0:T(8,128)S(1)}, s32[8,8]{1,0:T(8,128)S(1)}) fusion(s32[1,8,8]{2,1,0:T(8,128)} %param.15, s32[]{:T(128)S(6)} %axis_index.23), kind=kLoop, calls=%fused_computation.64 | loop fusion | flops 1408 | bytes 772 | tf_op jit(solution)/shard_map/jit(_where)/select_n | solution.py:57
  2.3 7.3 %all-to-all-start = ((s32[8,1,1]{2,1,0:T(1,128)}), s32[8,1,1]{2,1,0:T(1,128)S(1)}, u32[]{:S(2)}, u32[]{:S(2)}) async-start(s32[8,1,1]{2,1,0:T(1,128)} %copy.39), calls=%async_computation | async-start | bytes 8192 | tf_op jit(solution)/shard_map/all_to_all | solution.py:63
  10.4 1.7 %convolution_bitcast_fusion.1 = f32[512,1,64]{0,2,1:T(8,128)S(1)} fusion(bf16[512,2048]{1,0:T(8,128)(2,1)S(1)} %copy-done, bf16[2048,64]{0,1:T(8,128)(2,1)} %param.11), kind=kOutput, calls=%fused_computation.26 | convolution fusion | flops 134217728 | bytes 2490368 | tf_op jit(solution)/shard_map/dot_general | solution.py:47
  13.9 2.0 %fusion.34 = f32[512,256]{0,1:T(8,128)S(1)} fusion(bf16[512,2048]{1,0:T(8,128)(2,1)S(1)} %copy-done, bf16[2048,256]{1,0:T(8,128)(2,1)} %param.10), kind=kOutput, calls=%fused_computation.93 | convolution fusion | flops 536870912 | bytes 3670016 | tf_op jit(solution)/shard_map/dot_general | solution.py:40
  16.4 1.6 %pad_maximum_fusion = bf16[4,2,64,4,64]{2,1,0,4,3:T(2,128)(2,1)} fusion(bf16[4,2,64,4,32]{2,1,0,4,3:T(2,128)(2,1)S(1)} %concatenate.35, bf16[4,2,64,4,32]{2,1,0,4,3:T(2,128)(2,1)S(1)} %concatenate.34), kind=kLoop, calls=%fused_computation.29 | loop fusion | flops 131072 | bytes 524288 | tf_op jit(solution)/shard_map/concatenate | solution.py:22
  20.0 6.0 %all-to-all-start.1 = ((bf16[8,64,128]{2,1,0:T(8,128)(2,1)}), bf16[8,64,128]{2,1,0:T(8,128)(2,1)S(1)}, u32[]{:S(2)}, u32[]{:S(2)}) async-start(bf16[8,64,128]{2,1,0:T(8,128)(2,1)} %broadcast_select_fusion), calls=%async_computation.1 | async-start | bytes 262144 | tf_op jit(solution)/shard_map/all_to_all | solution.py:71
  26.8 6.5 %all-to-all-done.1 = bf16[8,64,128]{2,1,0:T(8,128)(2,1)S(1)} async-done(((bf16[8,64,128]{2,1,0:T(8,128)(2,1)}), bf16[8,64,128]{2,1,0:T(8,128)(2,1)S(1)}, u32[]{:S(2)}, u32[]{:S(2)}) %all-to-all-start.1) | async-done | bytes 131104 | tf_op jit(solution)/shard_map/all_to_all | solution.py:71
  34.3 17.1 %while.11 = (s32[]{:T(128)}, bf16[4,2,64,4,64]{2,4,3,1,0:T(8,128)(2,1)}, bf16[4,2,8,64,128]{4,3,2,1,0:T(8,128)(2,1)S(1)}, pred[4,2,8]{2,1,0:T(4,128)(4,1)S(1)}, ...) while((s32[]{:T(128)}, ...), condition=%wide.region_4.5_spmd.clone, body=%wide.region_1.4_spmd.clone.sunk | while | flops 69369872 | bytes 13193617 | solution.py:100
  35.3 1.0 %constant_dynamic-slice_fusion.4 = bf16[1,2,64,4,64]{2,1,0,4,3:T(2,128)(2,1)S(1)} fusion(bf16[4,2,64,4,64]{2,1,0,4,3:T(2,128)(2,1)} %get-tuple-element.185, s32[]{:T(128)} %get-tuple-element.171), kind=kLoop, calls=%fused_computation.18.clone.1 | loop fusion | bytes 131076 | tf_op jit(solution)/shard_map/while/body/jit(dynamic_index_in_dim)/dynamic_slice | solution.py:100
  37.3 1.2 %fusion.52 = bf16[4,2,64,4,64]{2,4,3,1,0:T(8,128)(2,1)} fusion(bf16[4,2,64,4,64]{2,4,3,1,0:T(8,128)(2,1)} %get-tuple-element.172, s32[]{:T(128)} %get-tuple-element.171, f32[2,4,64,8,64]{2,4,1,3,0:T(8,128)S(1)} %get-tuple-element.161, f32[2,4,64]{2,1,0:T(4,128)S(1)} %fusion.51, f32[2,4,64]{2,1,0:T(4,128)S(1)} %get-tuple-element.162, ...), kind=kOutput, calls=%fused_computation.10.clone.1 | convolution fusion | flops 34373632 | bytes 1446400 | tf_op jit(solution)/shard_map/while/body/eval_jaxpr/phqsk,pskd->pqhd/dot_general | solution.py:95
  39.6 1.0 %constant_dynamic-slice_fusion.4 = bf16[1,2,64,4,64]{2,1,0,4,3:T(2,128)(2,1)S(1)} fusion(bf16[4,2,64,4,64]{2,1,0,4,3:T(2,128)(2,1)} %get-tuple-element.185, s32[]{:T(128)} %get-tuple-element.171), kind=kLoop, calls=%fused_computation.18.clone.1 | loop fusion | bytes 131076 | tf_op jit(solution)/shard_map/while/body/jit(dynamic_index_in_dim)/dynamic_slice | solution.py:100
  41.6 1.2 %fusion.52 = bf16[4,2,64,4,64]{2,4,3,1,0:T(8,128)(2,1)} fusion(bf16[4,2,64,4,64]{2,4,3,1,0:T(8,128)(2,1)} %get-tuple-element.172, s32[]{:T(128)} %get-tuple-element.171, f32[2,4,64,8,64]{2,4,1,3,0:T(8,128)S(1)} %get-tuple-element.161, f32[2,4,64]{2,1,0:T(4,128)S(1)} %fusion.51, f32[2,4,64]{2,1,0:T(4,128)S(1)} %get-tuple-element.162, ...), kind=kOutput, calls=%fused_computation.10.clone.1 | convolution fusion | flops 34373632 | bytes 1446400 | tf_op jit(solution)/shard_map/while/body/eval_jaxpr/phqsk,pskd->pqhd/dot_general | solution.py:95
  43.8 1.0 %constant_dynamic-slice_fusion.4 = bf16[1,2,64,4,64]{2,1,0,4,3:T(2,128)(2,1)S(1)} fusion(bf16[4,2,64,4,64]{2,1,0,4,3:T(2,128)(2,1)} %get-tuple-element.185, s32[]{:T(128)} %get-tuple-element.171), kind=kLoop, calls=%fused_computation.18.clone.1 | loop fusion | bytes 131076 | tf_op jit(solution)/shard_map/while/body/jit(dynamic_index_in_dim)/dynamic_slice | solution.py:100
  45.9 1.2 %fusion.52 = bf16[4,2,64,4,64]{2,4,3,1,0:T(8,128)(2,1)} fusion(bf16[4,2,64,4,64]{2,4,3,1,0:T(8,128)(2,1)} %get-tuple-element.172, s32[]{:T(128)} %get-tuple-element.171, f32[2,4,64,8,64]{2,4,1,3,0:T(8,128)S(1)} %get-tuple-element.161, f32[2,4,64]{2,1,0:T(4,128)S(1)} %fusion.51, f32[2,4,64]{2,1,0:T(4,128)S(1)} %get-tuple-element.162, ...), kind=kOutput, calls=%fused_computation.10.clone.1 | convolution fusion | flops 34373632 | bytes 1446400 | tf_op jit(solution)/shard_map/while/body/eval_jaxpr/phqsk,pskd->pqhd/dot_general | solution.py:95
  48.1 1.0 %constant_dynamic-slice_fusion.4 = bf16[1,2,64,4,64]{2,1,0,4,3:T(2,128)(2,1)S(1)} fusion(bf16[4,2,64,4,64]{2,1,0,4,3:T(2,128)(2,1)} %get-tuple-element.185, s32[]{:T(128)} %get-tuple-element.171), kind=kLoop, calls=%fused_computation.18.clone.1 | loop fusion | bytes 131076 | tf_op jit(solution)/shard_map/while/body/jit(dynamic_index_in_dim)/dynamic_slice | solution.py:100
  50.2 1.2 %fusion.52 = bf16[4,2,64,4,64]{2,4,3,1,0:T(8,128)(2,1)} fusion(bf16[4,2,64,4,64]{2,4,3,1,0:T(8,128)(2,1)} %get-tuple-element.172, s32[]{:T(128)} %get-tuple-element.171, f32[2,4,64,8,64]{2,4,1,3,0:T(8,128)S(1)} %get-tuple-element.161, f32[2,4,64]{2,1,0:T(4,128)S(1)} %fusion.51, f32[2,4,64]{2,1,0:T(4,128)S(1)} %get-tuple-element.162, ...), kind=kOutput, calls=%fused_computation.10.clone.1 | convolution fusion | flops 34373632 | bytes 1446400 | tf_op jit(solution)/shard_map/while/body/eval_jaxpr/phqsk,pskd->pqhd/dot_general | solution.py:95
  51.4 1.3 %copy.44 = f32[4,2,64,4,64]{4,3,2,1,0:T(4,128)S(1)} copy(bf16[4,2,64,4,64]{2,4,3,1,0:T(8,128)(2,1)} %get-tuple-element.47) | data formatting | bytes 786432 | tf_op jit(solution)/shard_map/convert_element_type | solution.py:110
  52.7 1.4 %reshape.370 = f32[512,256]{1,0:T(8,128)} reshape(f32[4,2,64,4,64]{4,3,2,1,0:T(4,128)S(1)} %copy.44) | data formatting | bytes 1048576 | tf_op jit(solution)/shard_map/convert_element_type | solution.py:110
  54.1 1.1 %multiply_convert_fusion = bf16[512,256]{1,0:T(8,128)(2,1)S(1)} fusion(f32[512,256]{1,0:T(8,128)} %reshape.370, f32[256]{0:T(256)S(1)} %dynamic_slice.23), kind=kLoop, calls=%fused_computation.30 | loop fusion | flops 262144 | bytes 787456 | tf_op jit(solution)/shard_map/convert_element_type | solution.py:113
  55.4 1.1 %stack.2 = bf16[4,512,256]{1,2,0:T(8,128)(2,1)} broadcast(bf16[512,256]{0,1:T(8,128)(2,1)S(1)} %copy.45), dimensions={1,2} | broadcast | bytes 1310720 | tf_op jit(solution)/shard_map/stack | solution.py:116
  56.4 3.5 %all-to-all-start.2 = ((bf16[4,512,256]{1,2,0:T(8,128)(2,1)}), bf16[4,512,256]{1,2,0:T(8,128)(2,1)S(1)}, u32[]{:S(2)}, u32[]{:S(2)}) async-start(bf16[4,512,256]{1,2,0:T(8,128)(2,1)} %stack.2), calls=%async_computation.2 | async-start | bytes 2097152 | tf_op jit(solution)/shard_map/all_to_all | solution.py:116
  60.0 1.2 %multiply_reduce_fusion = f32[4,2,64]{2,1,0:T(2,128)S(1)} fusion(bf16[4,2,64,4,64]{2,4,3,1,0:T(8,128)(2,1)} %get-tuple-element.47), kind=kLoop, calls=%fused_computation.28 | loop fusion | flops 392704 | bytes 264192 | tf_op jit(solution)/shard_map/reduce_sum | solution.py:111
  61.3 14.6 %psum.7 = f32[512]{0:T(512)S(1)} all-reduce(f32[512]{0:T(512)S(1)} %reduce_sum.21), channel_id=1, replica_groups=mesh['kv'=8,'tp'=4] {'tp'}, use_global_device_ids=true, to_apply=%region_6.7 | all-reduce | flops 512 | bytes 4096 | tf_op jit(solution)/shard_map/psum | solution.py:111
  75.8 2.8 %fusion.10 = bf16[512,512]{1,0:T(8,128)(2,1)} fusion(bf16[512,1024]{0,1:T(8,128)(2,1)S(1)} %bitcast.158, bf16[1024,512]{1,0:T(8,128)(2,1)} %param.13, f32[512]{0:T(512)S(1)} %add_rsqrt_fusion), kind=kOutput, calls=%fused_computation.25 | convolution fusion | flops 537395200 | bytes 2623488 | tf_op jit(solution)/shard_map/dot_general | solution.py:114
  (92 shorter events, 16.3 us)
Async XLA Ops:
  0.0 10.4 %copy-start = (bf16[512,2048]{1,0:T(8,128)(2,1)S(1)}, bf16[512,2048]{1,0:T(8,128)(2,1)}, u32[]{:S(2)}) copy-start(bf16[512,2048]{1,0:T(8,128)(2,1)} %param.9) | copy-start | bytes 6291460
  0.0 13.0 %copy-start.3 = (bf16[2048,64]{0,1:T(8,128)(2,1)S(1)}, bf16[2048,64]{0,1:T(8,128)(2,1)}, u32[]{:S(2)}) copy-start(bf16[2048,64]{0,1:T(8,128)(2,1)} %param.12) | copy-start | bytes 786436
  2.3 15.9 %all-to-all-start = ((s32[8,1,1]{2,1,0:T(1,128)}), s32[8,1,1]{2,1,0:T(1,128)S(1)}, u32[]{:S(2)}, u32[]{:S(2)}) async-start(s32[8,1,1]{2,1,0:T(1,128)} %copy.39), calls=%async_computation | async-start | bytes 8192 | tf_op jit(solution)/shard_map/all_to_all | solution.py:63
  15.9 10.9 %copy-start.4 = (s32[1,8,8]{2,1,0:T(8,128)S(1)}, s32[1,8,8]{2,1,0:T(8,128)}, u32[]{:S(2)}) copy-start(s32[1,8,8]{2,1,0:T(8,128)} %param.15) | copy-start | bytes 772
  20.0 13.3 %all-to-all-start.1 = ((bf16[8,64,128]{2,1,0:T(8,128)(2,1)}), bf16[8,64,128]{2,1,0:T(8,128)(2,1)S(1)}, u32[]{:S(2)}, u32[]{:S(2)}) async-start(bf16[8,64,128]{2,1,0:T(8,128)(2,1)} %broadcast_select_fusion), calls=%async_computation.1 | async-start | bytes 262144 | tf_op jit(solution)/shard_map/all_to_all | solution.py:71
  34.3 1.0 %copy-start.1 = (bf16[4,2,8,64,128]{4,3,2,1,0:T(8,128)(2,1)}, bf16[4,2,8,64,128]{4,3,2,1,0:T(8,128)(2,1)S(1)}, u32[]{:S(2)}) copy-start(bf16[4,2,8,64,128]{4,3,2,1,0:T(8,128)(2,1)S(1)} %get-tuple-element.181) | copy-start | bytes 3145732 | tf_op jit(solution)/shard_map/while
  37.3 1.2 %copy-start.2 = (bf16[4,2,8,64,128]{4,3,2,1,0:T(8,128)(2,1)S(1)}, bf16[4,2,8,64,128]{4,3,2,1,0:T(8,128)(2,1)}, u32[]{:S(2)}) copy-start(bf16[4,2,8,64,128]{4,3,2,1,0:T(8,128)(2,1)} %copy-done.1) | copy-start | bytes 3145732 | tf_op jit(solution)/shard_map/while
  38.6 1.0 %copy-start.1 = (bf16[4,2,8,64,128]{4,3,2,1,0:T(8,128)(2,1)}, bf16[4,2,8,64,128]{4,3,2,1,0:T(8,128)(2,1)S(1)}, u32[]{:S(2)}) copy-start(bf16[4,2,8,64,128]{4,3,2,1,0:T(8,128)(2,1)S(1)} %get-tuple-element.181) | copy-start | bytes 3145732 | tf_op jit(solution)/shard_map/while
  41.6 1.2 %copy-start.2 = (bf16[4,2,8,64,128]{4,3,2,1,0:T(8,128)(2,1)S(1)}, bf16[4,2,8,64,128]{4,3,2,1,0:T(8,128)(2,1)}, u32[]{:S(2)}) copy-start(bf16[4,2,8,64,128]{4,3,2,1,0:T(8,128)(2,1)} %copy-done.1) | copy-start | bytes 3145732 | tf_op jit(solution)/shard_map/while
  42.9 1.0 %copy-start.1 = (bf16[4,2,8,64,128]{4,3,2,1,0:T(8,128)(2,1)}, bf16[4,2,8,64,128]{4,3,2,1,0:T(8,128)(2,1)S(1)}, u32[]{:S(2)}) copy-start(bf16[4,2,8,64,128]{4,3,2,1,0:T(8,128)(2,1)S(1)} %get-tuple-element.181) | copy-start | bytes 3145732 | tf_op jit(solution)/shard_map/while
  45.9 1.2 %copy-start.2 = (bf16[4,2,8,64,128]{4,3,2,1,0:T(8,128)(2,1)S(1)}, bf16[4,2,8,64,128]{4,3,2,1,0:T(8,128)(2,1)}, u32[]{:S(2)}) copy-start(bf16[4,2,8,64,128]{4,3,2,1,0:T(8,128)(2,1)} %copy-done.1) | copy-start | bytes 3145732 | tf_op jit(solution)/shard_map/while
  47.1 1.0 %copy-start.1 = (bf16[4,2,8,64,128]{4,3,2,1,0:T(8,128)(2,1)}, bf16[4,2,8,64,128]{4,3,2,1,0:T(8,128)(2,1)S(1)}, u32[]{:S(2)}) copy-start(bf16[4,2,8,64,128]{4,3,2,1,0:T(8,128)(2,1)S(1)} %get-tuple-element.181) | copy-start | bytes 3145732 | tf_op jit(solution)/shard_map/while
  50.2 1.2 %copy-start.2 = (bf16[4,2,8,64,128]{4,3,2,1,0:T(8,128)(2,1)S(1)}, bf16[4,2,8,64,128]{4,3,2,1,0:T(8,128)(2,1)}, u32[]{:S(2)}) copy-start(bf16[4,2,8,64,128]{4,3,2,1,0:T(8,128)(2,1)} %copy-done.1) | copy-start | bytes 3145732 | tf_op jit(solution)/shard_map/while
  56.4 19.4 %all-to-all-start.2 = ((bf16[4,512,256]{1,2,0:T(8,128)(2,1)}), bf16[4,512,256]{1,2,0:T(8,128)(2,1)S(1)}, u32[]{:S(2)}, u32[]{:S(2)}) async-start(bf16[4,512,256]{1,2,0:T(8,128)(2,1)} %stack.2), calls=%async_computation.2 | async-start | bytes 2097152 | tf_op jit(solution)/shard_map/all_to_all | solution.py:116
